TPU v7x, 32 devices: a whole 2x2x4 slice. The times are simulated.
32 devices in a mesh: tp: 32 (over z, y, x, core).
Axes of the slice: x: 2, y: 2, z: 4, core: 2. Of those that a mesh axis runs over, the one named last changes fastest.
Arguments:
- tokens: bfloat16 [32, 4096], replicated, may hold values from -18 to 18
- norm_gain: float32 [2, 4096], replicated, may hold values from 0.1 to 1.9
- w_gate: bfloat16 [2, 4096, 8192], P(None, None, 'tp'), may hold values from -0.09375 to 0.09375
- w_value: bfloat16 [2, 4096, 8192], P(None, None, 'tp'), may hold values from -0.09375 to 0.09375
- w_write: bfloat16 [2, 4096, 1024], P(None, None, 'tp'), may hold values from -0.09375 to 0.09375
- w_read: bfloat16 [2, 4096, 1024], P(None, None, 'tp'), may hold values from -0.09375 to 0.09375
- w_step: bfloat16 [2, 4096, 128], replicated, may hold values from -0.09375 to 0.09375
- step_bias: float32 [2, 128], replicated, may hold values from -2 to 1
- decay_rate: float32 [2, 128], replicated, may hold values from 0.05 to 3
- skip_gain: float32 [2, 128], replicated, may hold values from 1 to 4
- conv_value_weight: float32 [2, 3, 8192], P(None, None, 'tp'), may hold values from -2.5 to 2.5
- conv_key_weight: float32 [2, 3, 2, 1024], P(None, None, None, 'tp'), may hold values from -2.5 to 2.5
- group_gain: float32 [2, 8192], P(None, 'tp'), may hold values from 0.1 to 1.9
- w_out: bfloat16 [2, 8192, 4096], P(None, 'tp'), may hold values from -0.0625 to 0.0625
- ssm_state: float32 [2, 32, 8192, 128], P(None, None, 'tp'), may hold values from -3 to 3
- conv_value: float32 [2, 32, 2, 8192], P(None, None, None, 'tp'), may hold values from -5 to 5
- conv_key: float32 [2, 32, 2, 2, 1024], P(None, None, None, None, 'tp'), may hold values from -5 to 5
Outputs:
- tokens_out: bfloat16 [32, 4096], replicated
- ssm_state_out: float32 [2, 32, 8192, 128], P(None, None, 'tp')
- conv_value_out: float32 [2, 32, 2, 8192], P(None, None, None, 'tp')
- conv_key_out: float32 [2, 32, 2, 2, 1024], P(None, None, None, None, 'tp')
All inputs are finite; a program needn't handle non-finite values.
Results may differ from a plain program's by a relative error of at most 0.011.
Values may be sent and summed in bfloat16 or wider, within the bound.
A program may use at most 128 MiB of HBM per device.

v0:
```python
import jax
import jax.numpy as jnp
from jax import lax
from jax.sharding import PartitionSpec as P

D = 4096
HEAD_DIM = 64
GROUPS = 8
STATE = 128
LAYERS = 2
HEADS = 128
GW = 1024
EPS = 1e-06


def per_device(
    tokens,
    norm_gain,
    w_gate,
    w_value,
    w_write,
    w_read,
    w_step,
    step_bias,
    decay_rate,
    skip_gain,
    conv_value_weight,
    conv_key_weight,
    group_gain,
    w_out,
    ssm_state,
    conv_value,
    conv_key,
):
    highest = lax.Precision.HIGHEST
    chan_count = w_gate.shape[2]
    position = lax.axis_index("tp")
    first_chan = position * chan_count
    chan_ids = first_chan + jnp.arange(chan_count, dtype=jnp.int32)
    my_group = first_chan // GW
    head_hot = (
        (chan_ids // HEAD_DIM)[:, None] == jnp.arange(HEADS, dtype=jnp.int32)[None, :]
    ).astype(jnp.float32)
    group_hot = ((chan_ids // GW)[:, None] == jnp.arange(GROUPS, dtype=jnp.int32)[None, :]).astype(
        jnp.float32
    )
    hidden = tokens
    ssm_list = []
    value_list = []
    key_list = []
    for layer in range(LAYERS):
        resid = hidden.astype(jnp.float32)
        inv_scale = lax.rsqrt(jnp.sum(resid * resid, axis=1) / D + EPS)[:, None]
        scaled = (resid * norm_gain[layer]).astype(jnp.bfloat16)

        def project(weight):
            return jnp.dot(scaled, weight[layer], preferred_element_type=jnp.float32) * inv_scale

        gate_in = project(w_gate)
        value_in = project(w_value)
        write_in = project(w_write)
        read_in = project(w_read)
        step_in = project(w_step)
        value_window = jnp.concatenate([conv_value[layer], value_in[:, None, :]], axis=1)
        value_list.append(value_window[:, 1:])
        values = jax.nn.silu(jnp.sum(value_window * conv_value_weight[layer][None], axis=1))
        fresh = jnp.stack([write_in, read_in], axis=1)[:, None]
        key_window = jnp.concatenate([conv_key[layer], fresh], axis=1)
        key_list.append(key_window[:, 1:])
        mixed_keys = jax.nn.silu(jnp.sum(key_window * conv_key_weight[layer][None], axis=1))
        every_group = lax.all_gather(mixed_keys, "tp", axis=2, tiled=True)
        by_entry = every_group.reshape(every_group.shape[0], 2, STATE, GROUPS)
        own_keys = lax.dynamic_slice_in_dim(by_entry, my_group, 1, 3)[..., 0]
        writes = own_keys[:, 0]
        reads = own_keys[:, 1]
        delta = jax.nn.softplus(step_in + step_bias[layer][None])
        decay = jnp.exp(-delta * decay_rate[layer][None])
        delta_chan = jnp.dot(delta, head_hot.T, precision=highest)
        decay_chan = jnp.dot(decay, head_hot.T, precision=highest)
        skip_chan = jnp.dot(skip_gain[layer], head_hot.T, precision=highest)
        state = (
            decay_chan[..., None] * ssm_state[layer]
            + (delta_chan * values)[..., None] * writes[:, None, :]
        )
        ssm_list.append(state)
        read_out = jnp.sum(state * reads[:, None, :], axis=2) + skip_chan[None] * values
        gated = read_out * jax.nn.silu(gate_in)
        squares = jnp.dot(gated * gated, group_hot, precision=highest)
        square_total = lax.psum(squares, "tp")
        group_scale = lax.rsqrt(square_total / GW + EPS)
        scale_chan = jnp.dot(group_scale, group_hot.T, precision=highest)
        normed = (gated * scale_chan * group_gain[layer][None]).astype(jnp.bfloat16)
        partial_out = jnp.dot(normed, w_out[layer], preferred_element_type=jnp.float32)
        update = lax.psum(partial_out, "tp")
        hidden = (resid + update).astype(jnp.bfloat16)
    return (hidden, jnp.stack(ssm_list), jnp.stack(value_list), jnp.stack(key_list))


def solution(mesh):
    placed = (
        P(),
        P(),
        P(None, None, "tp"),
        P(None, None, "tp"),
        P(None, None, "tp"),
        P(None, None, "tp"),
        P(),
        P(),
        P(),
        P(),
        P(None, None, "tp"),
        P(None, None, None, "tp"),
        P(None, "tp"),
        P(None, "tp", None),
        P(None, None, "tp", None),
        P(None, None, None, "tp"),
        P(None, None, None, None, "tp"),
    )
    return jax.shard_map(
        per_device,
        mesh=mesh,
        in_specs=placed,
        out_specs=(
            P(),
            P(None, None, "tp", None),
            P(None, None, None, "tp"),
            P(None, None, None, None, "tp"),
        ),
        check_vma=False,
    )
```

profile of v0, /device:TPU:0, one launch (start us, length us, event | category | flops | bytes accessed | tf_op | source)
XLA Modules:
  0.0 486.0 jit_solution(18059725305354858468)
XLA Ops:
  7.2 0.0 copy-start
  7.2 0.0 all-reduce.3.cloned.1.call-start
  7.3 1.3 fusion.57
  8.6 0.8 slice_bitcast_fusion.11
  9.3 0.8 slice_bitcast_fusion.10
  10.1 0.8 fusion.160
  10.9 0.8 fusion.159
  11.6 0.7 slice_bitcast_fusion.8
  12.3 0.9 fusion.158
  13.2 1.2 fusion.51
  14.4 1.2 fusion.50
  15.8 2.1 fusion.29
  18.0 0.1 fusion.77
  18.1 0.0 copy-done.5
  18.1 0.3 compare_select_fusion.1
  18.4 0.3 fusion.79
  18.7 0.1 fusion.73
  18.8 0.3 convolution_multiply_fusion.3
  19.1 0.1 fusion.92
  19.3 0.1 copy.61
  19.3 46.2 %all_gather.6 = f32[32,2,1024]{0,1,2:T(2,128)S(1)} all-gather(f32[32,2,32]{0,1,2:T(2,128)S(1)} %copy.61), channel_id=1, replica_groups=mesh['tp'=32] {'tp'}, dimensions={2}, use_global_device_ids=true | all-gather | bytes 270336 | tf_op jit(solution)/shard_map/all_gather | solution.py:71
  65.5 0.1 copy.80
  65.6 0.1 constant_dynamic-slice_fusion.1
  65.7 0.1 copy.63
  65.8 5.5 %fusion.5 = f32[32,256]{1,0:T(8,128)S(1)} fusion(f32[2,32,256,128]{3,2,1,0:T(8,128)} %param.31, f32[32,128]{1,0:T(8,128)S(1)} %get-tuple-element.17, f32[32,128]{1,0:T(8,128)S(1)} %get-tuple-element.16, f32[32,256]{1,0:T(8,128)S(1)} %convolution_multiply_fusion.3, f32[32,256]{1,0:T(8,128)S(1)} %fusion.79), kind=kLoop, calls=%fused_computation.8 | loop fusion | flops 5234688 | bytes 4325376 | tf_op jit(solution)/shard_map/reduce_sum | solution.py:86
  71.4 0.4 multiply_multiply_fusion.1
  71.8 0.3 fusion.75
  72.1 36.8 %psum.28 = f32[32,8]{0,1:T(8,128)S(1)} all-reduce(f32[32,8]{0,1:T(8,128)S(1)} %fusion.75), channel_id=1, replica_groups=mesh['tp'=32] {'tp'}, use_global_device_ids=true, to_apply=%region_4.5 | all-reduce | flops 256 | bytes 2048 | tf_op jit(solution)/shard_map/psum | solution.py:89
  108.9 0.3 fusion.44
  109.2 2.9 fusion.12
  112.1 0.0 all-reduce.3.cloned.1.call-update
  112.1 0.0 all-reduce.5.cloned.1.call-start
  112.2 0.1 fusion.101
  112.3 0.1 fusion.76
  112.4 129.4 %all-reduce.3.cloned.1.call-done = f32[32,4096]{1,0:T(8,128)} async-done(((f32[32,4096]{1,0:T(8,128)}), f32[32,4096]{1,0:T(8,128)}) %all-reduce.3.cloned.1.call-update) | async-done | bytes 524304 | tf_op jit(solution)/shard_map/psum | solution.py:94
  241.8 1.2 fusion.60
  243.0 0.2 fusion.48
  243.2 0.0 copy-done.7
  243.3 0.2 fusion.49
  243.5 2.0 fusion.38
  245.5 1.5 compare_select_fusion
  247.1 0.1 fusion.93
  247.3 0.1 copy.68
  247.4 0.1 fusion.99
  247.5 0.1 fusion.71
  247.6 0.3 fusion.78
  247.9 0.3 convolution_multiply_fusion.1
  248.1 42.5 %all_gather.7 = f32[32,2,1024]{0,1,2:T(2,128)S(1)} all-gather(f32[32,2,32]{0,1,2:T(2,128)S(1)} %copy.68), channel_id=1, replica_groups=mesh['tp'=32] {'tp'}, dimensions={2}, use_global_device_ids=true | all-gather | bytes 270336 | tf_op jit(solution)/shard_map/all_gather | solution.py:71
  290.6 0.1 copy.79
  290.7 0.1 constant_dynamic-slice_fusion
  290.8 0.1 copy.70
  290.9 10.5 %multiply_add_fusion.1 = (f32[1,32,256,128]{3,2,1,0:T(8,128)}, f32[1,32,256,128]{3,2,1,0:T(8,128)}) fusion(f32[2,32,256,128]{3,2,1,0:T(8,128)} %param.31, f32[32,128]{1,0:T(8,128)S(1)} %get-tuple-element.16, f32[32,256]{1,0:T(8,128)S(1)} %convolution_multiply_fusion.3, f32[32,256]{1,0:T(8,128)S(1)} %fusion.79, f32[32,128]{1,0:T(8,128)S(1)} %get-tuple-element.12, ...), kind=kLoop, calls=%fused_computation.10 | loop fusion | flops 6291456 | bytes 16941056 | tf_op jit(solution)/shard_map/add | solution.py:82
  301.4 5.5 %fusion.2 = f32[32,256]{1,0:T(8,128)S(1)} fusion(f32[2,32,256,128]{3,2,1,0:T(8,128)} %param.31, f32[32,128]{1,0:T(8,128)S(1)} %get-tuple-element.13, f32[32,128]{1,0:T(8,128)S(1)} %get-tuple-element.12, f32[32,256]{1,0:T(8,128)S(1)} %convolution_multiply_fusion.1, f32[32,256]{1,0:T(8,128)S(1)} %fusion.78), kind=kLoop, calls=%fused_computation.4 | loop fusion | flops 5234688 | bytes 4325376 | tf_op jit(solution)/shard_map/reduce_sum | solution.py:86
  306.9 0.4 multiply_multiply_fusion
  307.3 0.3 fusion.74
  307.6 36.8 %psum.30 = f32[32,8]{0,1:T(8,128)S(1)} all-reduce(f32[32,8]{0,1:T(8,128)S(1)} %fusion.74), channel_id=1, replica_groups=mesh['tp'=32] {'tp'}, use_global_device_ids=true, to_apply=%region_10.11 | all-reduce | flops 256 | bytes 2048 | tf_op jit(solution)/shard_map/psum | solution.py:89
  344.5 0.3 fusion.45
  344.7 2.9 fusion.6
  347.7 0.0 all-reduce.5.cloned.1.call-update
  347.7 0.7 pad_maximum_fusion.4
  348.4 0.7 pad_maximum_fusion.3
  349.1 7.9 %pad_maximum_fusion = f32[2,32,256,128]{3,2,1,0:T(8,128)} fusion(f32[1,32,256,128]{3,2,1,0:T(8,128)} %get-tuple-element.7, f32[1,32,256,128]{3,2,1,0:T(8,128)} %get-tuple-element.6), kind=kLoop, calls=%fused_computation | loop fusion | flops 2097152 | bytes 16777216 | tf_op jit(solution)/shard_map/stack | solution.py:96
  357.0 120.4 %all-reduce.5.cloned.1.call-done = f32[32,4096]{1,0:T(8,128)} async-done(((f32[32,4096]{1,0:T(8,128)}), f32[32,4096]{1,0:T(8,128)}) %all-reduce.5.cloned.1.call-update) | async-done | bytes 524304 | tf_op jit(solution)/shard_map/psum | solution.py:94
  477.4 1.8 fusion.61
  (34 shorter events, 0.4 us)
Async XLA Ops:
  7.2 10.9 %copy-start = (bf16[32,4096]{1,0:T(8,128)(2,1)S(1)}, bf16[32,4096]{1,0:T(8,128)(2,1)}, u32[]{:S(2)}) copy-start(bf16[32,4096]{1,0:T(8,128)(2,1)} %param.17) | copy-start | bytes 786436
  7.2 10.7 %copy-start.1 = (f32[2,32,2,256]{3,2,1,0:T(2,128)S(1)}, f32[2,32,2,256]{3,2,1,0:T(2,128)}, u32[]{:S(2)}) copy-start(f32[2,32,2,256]{3,2,1,0:T(2,128)} %param.32) | copy-start | bytes 393220
  7.2 10.8 %copy-start.8 = (f32[2,128]{1,0:T(2,128)S(1)}, f32[2,128]{1,0:T(2,128)}, u32[]{:S(2)}) copy-start(f32[2,128]{1,0:T(2,128)} %param.26) | copy-start | bytes 3076
  7.2 11.9 %copy-start.2 = (f32[2,32,2,2,32]{4,3,2,1,0:T(2,128)S(1)}, f32[2,32,2,2,32]{4,3,2,1,0:T(2,128)}, u32[]{:S(2)}) copy-start(f32[2,32,2,2,32]{4,3,2,1,0:T(2,128)} %param.33) | copy-start | bytes 98308
  7.2 234.6 %all-reduce.3.cloned.1.call-start = ((), (), s32[]{:S(2)}) async-start(), calls=%async_computation | async-start | bytes 1048576 | tf_op jit(solution)/shard_map/psum | solution.py:94
  7.3 10.8 %copy-start.5 = (bf16[2,4096,128]{2,1,0:T(8,128)(2,1)S(1)}, bf16[2,4096,128]{2,1,0:T(8,128)(2,1)}, u32[]{:S(2)}) copy-start(bf16[2,4096,128]{2,1,0:T(8,128)(2,1)} %param.23) | copy-start | bytes 6291460
  65.8 5.6 %copy-start.3 = (bf16[2,4096,256]{2,1,0:T(8,128)(2,1)S(1)}, bf16[2,4096,256]{2,1,0:T(8,128)(2,1)}, u32[]{:S(2)}) copy-start(bf16[2,4096,256]{2,1,0:T(8,128)(2,1)} %param.19) | copy-start | bytes 12582916
  71.3 171.7 %copy-start.6 = (bf16[2,4096,32]{1,2,0:T(8,128)(2,1)S(1)}, bf16[2,4096,32]{1,2,0:T(8,128)(2,1)}, u32[]{:S(2)}) copy-start(bf16[2,4096,32]{1,2,0:T(8,128)(2,1)} %param.22) | copy-start | bytes 1572868
  71.3 171.9 %copy-start.7 = (bf16[2,4096,32]{1,2,0:T(8,128)(2,1)S(1)}, bf16[2,4096,32]{1,2,0:T(8,128)(2,1)}, u32[]{:S(2)}) copy-start(bf16[2,4096,32]{1,2,0:T(8,128)(2,1)} %param.21) | copy-start | bytes 1572868
  112.1 365.3 %all-reduce.5.cloned.1.call-start = ((), (), s32[]{:S(2)}) async-start(), calls=%async_computation.1 | async-start | bytes 1048576 | tf_op jit(solution)/shard_map/psum | solution.py:94
  301.4 5.5 %copy-start.4 = (bf16[2,4096,256]{2,1,0:T(8,128)(2,1)S(1)}, bf16[2,4096,256]{2,1,0:T(8,128)(2,1)}, u32[]{:S(2)}) copy-start(bf16[2,4096,256]{2,1,0:T(8,128)(2,1)} %param.19) | copy-start | bytes 12582916
Sparse Core Ops, SparseCore 0:
  112.2 129.5 all-reduce.2
  347.8 129.4 all-reduce.4
where the time goes:
time: 487 us; the launch traced here: 486 us
  waiting for transfers between devices  250 us (51%)
  blocking collectives  162 us (33%)
  other arithmetic  35.8 us (7%)
  matrix products  18 us (4%)
  between operations  14.5 us (3%)
  local copies, waits for them, and re-layouts  5.49 us (1%)
    psum x2, waiting for transfers between devices, per_device(): update = lax.psum(partial_out, 'tp')  250 us
    all_gather x2, blocking collectives, per_device(): every_group = lax.all_gather(mixed_keys, 'tp', axis=2, tiled=True)  88.7 us
    psum x2, blocking collectives, per_device(): square_total = lax.psum(squares, 'tp')  73.6 us
    reduce_sum x2, other arithmetic, per_device(): jnp.sum(state * reads[:, None, :], axis=2) + skip_chan[None] * values  11 us
    add x1, other arithmetic, per_device(): decay_chan[..., None] * ssm_state[layer]  10.5 us
  transfers between devices with their start and end apart: 2, of which 2 were waited for; matrix products, arithmetic and copies ran while one was open for 2% of the time, Pallas kernels for 0%

commit v1 on v0

--- a/solution.py
+++ b/solution.py
@@ -91,7 +91,11 @@
         scale_chan = jnp.dot(group_scale, group_hot.T, precision=highest)
         normed = (gated * scale_chan * group_gain[layer][None]).astype(jnp.bfloat16)
         partial_out = jnp.dot(normed, w_out[layer], preferred_element_type=jnp.float32)
-        update = lax.psum(partial_out, "tp")
+        devices = lax.axis_size("tp")
+        update, far = (partial_out, 1)
+        while far < devices:
+            update = update + lax.ppermute(update, "tp", [(i, i ^ far) for i in range(devices)])
+            far = 2 * far
         hidden = (resid + update).astype(jnp.bfloat16)
     return (hidden, jnp.stack(ssm_list), jnp.stack(value_list), jnp.stack(key_list))
 

time: 487 us -> 332 us (0.68)
  waiting for transfers between devices: 250 us -> 104 us
  starting transfers between devices: 0.08 us -> 18 us
  between operations: 14.5 us -> 1.2 us
  other arithmetic: 35.8 us -> 28.1 us
    psum x2 -> x0, waiting for transfers between devices: 250 us -> none  [per_device(): update = lax.psum(partial_out, 'tp')]
    ppermute x0 -> x10, waiting for transfers between devices: none -> 104 us  [per_device(): lax.ppermute(update, 'tp', [(i, i ^ far) for i in range(devices)])]
    ppermute x0 -> x10, starting transfers between devices: none -> 18 us  [per_device(): lax.ppermute(update, 'tp', [(i, i ^ far) for i in range(devices)])]
  transfers between devices with their start and end apart: 2 -> 10, of which waited for: 2 -> 10; matrix products, arithmetic and copies ran while one was open for 2% -> 4% of each run, Pallas kernels for 0% -> 0%
where the time goes in v1:
time: 332 us; the launch traced here: 331 us
  blocking collectives  161 us (48%)
  waiting for transfers between devices  104 us (31%)
  other arithmetic  28.1 us (8%)
  starting transfers between devices  18 us (5%)
  matrix products  13.5 us (4%)
  local copies, waits for them, and re-layouts  5.52 us (2%)
    ppermute x10, waiting for transfers between devices, per_device(): lax.ppermute(update, 'tp', [(i, i ^ far) for i in range(devices)])  104 us
    all_gather x2, blocking collectives, per_device(): every_group = lax.all_gather(mixed_keys, 'tp', axis=2, tiled=True)  87.1 us
    psum x2, blocking collectives, per_device(): square_total = lax.psum(squares, 'tp')  73.6 us
    ppermute x10, starting transfers between devices, per_device(): lax.ppermute(update, 'tp', [(i, i ^ far) for i in range(devices)])  18 us
    reduce_sum x2, other arithmetic, per_device(): jnp.sum(state * reads[:, None, :], axis=2) + skip_chan[None] * values  11.1 us
    add x1, other arithmetic, per_device(): decay_chan[..., None] * ssm_state[layer]  8.16 us
    dot_general x10, matrix products, project(): jnp.dot(scaled, weight[layer], preferred_element_type=jnp.float32)  6.84 us
  transfers between devices with their start and end apart: 10, of which 10 were waited for; matrix products, arithmetic and copies ran while one was open for 4% of the time, Pallas kernels for 0%

profile of v1, /device:TPU:0, one launch (start us, length us, event | category | flops | bytes accessed | tf_op | source)
XLA Modules:
  0.0 330.7 jit_solution(9037258707302722763)
XLA Ops:
  0.7 1.3 fusion.57
  2.0 0.8 slice_bitcast_fusion.11
  2.8 0.8 slice_bitcast_fusion.10
  3.5 0.8 fusion.160
  4.3 0.8 fusion.159
  5.1 0.7 slice_bitcast_fusion.8
  5.8 0.9 fusion.158
  6.6 1.2 fusion.51
  7.8 1.3 fusion.50
  9.2 2.1 fusion.29
  11.4 0.1 fusion.77
  11.5 0.3 compare_select_fusion.1
  11.8 0.3 fusion.79
  12.1 0.1 fusion.73
  12.3 0.3 convolution_multiply_fusion.3
  12.8 46.2 %all_gather.6 = f32[32,2,1024]{0,1,2:T(2,128)S(1)} all-gather(f32[32,2,32]{0,1,2:T(2,128)S(1)} %copy.61), channel_id=1, replica_groups=mesh['tp'=32] {'tp'}, dimensions={2}, use_global_device_ids=true | all-gather | bytes 270336 | tf_op jit(solution)/shard_map/all_gather | solution.py:71
  59.0 0.1 constant_dynamic-slice_fusion.1
  59.2 5.5 %fusion.5 = f32[32,256]{1,0:T(8,128)S(1)} fusion(f32[2,32,256,128]{3,2,1,0:T(8,128)} %param.31, f32[32,128]{1,0:T(8,128)S(1)} %get-tuple-element.17, f32[32,128]{1,0:T(8,128)S(1)} %get-tuple-element.16, f32[32,256]{1,0:T(8,128)S(1)} %convolution_multiply_fusion.3, f32[32,256]{1,0:T(8,128)S(1)} %fusion.79), kind=kLoop, calls=%fused_computation.8 | loop fusion | flops 5234688 | bytes 4325376 | tf_op jit(solution)/shard_map/reduce_sum | solution.py:86
  64.8 0.4 multiply_multiply_fusion.1
  65.2 0.3 fusion.75
  65.5 36.8 %psum.14 = f32[32,8]{0,1:T(8,128)S(1)} all-reduce(f32[32,8]{0,1:T(8,128)S(1)} %fusion.75), channel_id=1, replica_groups=mesh['tp'=32] {'tp'}, use_global_device_ids=true, to_apply=%region_4.5 | all-reduce | flops 256 | bytes 2048 | tf_op jit(solution)/shard_map/psum | solution.py:89
  102.3 0.3 fusion.44
  102.6 2.0 fusion.12
  104.8 1.9 collective-permute-done
  106.7 0.1 add.167
  106.8 2.3 collective-permute-start.1
  109.1 12.2 %collective-permute-done.1 = f32[32,4096]{1,0:T(8,128)S(1)} collective-permute-done((f32[32,4096]{1,0:T(8,128)S(1)}, f32[32,4096]{1,0:T(8,128)S(1)}, u32[]{:S(2)}, u32[]{:S(2)}) %collective-permute-start.1) | collective-permute-done | bytes 524320 | tf_op jit(solution)/shard_map/ppermute | solution.py:97
  121.4 1.8 collective-permute-start.2
  123.2 11.7 %collective-permute-done.2 = f32[32,4096]{1,0:T(8,128)S(1)} collective-permute-done((f32[32,4096]{1,0:T(8,128)S(1)}, f32[32,4096]{1,0:T(8,128)S(1)}, u32[]{:S(2)}, u32[]{:S(2)}) %collective-permute-start.2) | collective-permute-done | bytes 524320 | tf_op jit(solution)/shard_map/ppermute | solution.py:97
  134.9 2.9 collective-permute-start.3
  137.9 10.8 %collective-permute-done.3 = f32[32,4096]{1,0:T(8,128)S(1)} collective-permute-done((f32[32,4096]{1,0:T(8,128)S(1)}, f32[32,4096]{1,0:T(8,128)S(1)}, u32[]{:S(2)}, u32[]{:S(2)}) %collective-permute-start.3) | collective-permute-done | bytes 524320 | tf_op jit(solution)/shard_map/ppermute | solution.py:97
  148.7 1.9 collective-permute-start.4
  150.6 0.1 fusion.76
  150.7 22.1 %collective-permute-done.4 = f32[32,4096]{1,0:T(8,128)S(1)} collective-permute-done((f32[32,4096]{1,0:T(8,128)S(1)}, f32[32,4096]{1,0:T(8,128)S(1)}, u32[]{:S(2)}, u32[]{:S(2)}) %collective-permute-start.4) | collective-permute-done | bytes 524320 | tf_op jit(solution)/shard_map/ppermute | solution.py:97
  172.9 0.2 fusion.60
  173.1 0.2 fusion.48
  173.3 0.2 fusion.49
  173.6 0.4 fusion.38
  174.0 0.3 compare_select_fusion
  174.6 0.3 fusion.78
  174.9 0.1 fusion.71
  175.0 0.3 convolution_multiply_fusion.1
  175.3 40.9 %all_gather.7 = f32[32,2,1024]{0,1,2:T(2,128)S(1)} all-gather(f32[32,2,32]{0,1,2:T(2,128)S(1)} %copy.68), channel_id=1, replica_groups=mesh['tp'=32] {'tp'}, dimensions={2}, use_global_device_ids=true | all-gather | bytes 270336 | tf_op jit(solution)/shard_map/all_gather | solution.py:71
  216.2 0.1 constant_dynamic-slice_fusion
  216.4 5.5 %fusion.2 = f32[32,256]{1,0:T(8,128)S(1)} fusion(f32[2,32,256,128]{3,2,1,0:T(8,128)} %param.31, f32[32,128]{1,0:T(8,128)S(1)} %get-tuple-element.13, f32[32,128]{1,0:T(8,128)S(1)} %get-tuple-element.12, f32[32,256]{1,0:T(8,128)S(1)} %convolution_multiply_fusion.1, f32[32,256]{1,0:T(8,128)S(1)} %fusion.78), kind=kLoop, calls=%fused_computation.4 | loop fusion | flops 5234688 | bytes 4325376 | tf_op jit(solution)/shard_map/reduce_sum | solution.py:86
  222.0 0.4 multiply_multiply_fusion
  222.4 0.3 fusion.74
  222.7 36.8 %psum.15 = f32[32,8]{0,1:T(8,128)S(1)} all-reduce(f32[32,8]{0,1:T(8,128)S(1)} %fusion.74), channel_id=1, replica_groups=mesh['tp'=32] {'tp'}, use_global_device_ids=true, to_apply=%region_9.10 | all-reduce | flops 256 | bytes 2048 | tf_op jit(solution)/shard_map/psum | solution.py:89
  259.5 0.3 fusion.45
  259.8 2.1 fusion.6
  261.9 1.9 collective-permute-done.5
  263.9 2.3 collective-permute-start.6
  266.2 12.2 %collective-permute-done.6 = f32[32,4096]{1,0:T(8,128)S(1)} collective-permute-done((f32[32,4096]{1,0:T(8,128)S(1)}, f32[32,4096]{1,0:T(8,128)S(1)}, u32[]{:S(2)}, u32[]{:S(2)}) %collective-permute-start.6) | collective-permute-done | bytes 524320 | tf_op jit(solution)/shard_map/ppermute | solution.py:97
  278.5 1.8 collective-permute-start.7
  280.5 0.7 pad_maximum_fusion.4
  281.2 10.8 %collective-permute-done.7 = f32[32,4096]{1,0:T(8,128)S(1)} collective-permute-done((f32[32,4096]{1,0:T(8,128)S(1)}, f32[32,4096]{1,0:T(8,128)S(1)}, u32[]{:S(2)}, u32[]{:S(2)}) %collective-permute-start.7) | collective-permute-done | bytes 524320 | tf_op jit(solution)/shard_map/ppermute | solution.py:97
  292.0 2.9 collective-permute-start.8
  295.0 8.2 %multiply_add_fusion.1 = (f32[1,32,256,128]{3,2,1,0:T(8,128)S(1)}, f32[1,32,256,128]{3,2,1,0:T(8,128)S(1)}) fusion(f32[2,32,256,128]{3,2,1,0:T(8,128)} %param.31, f32[32,128]{1,0:T(8,128)S(1)} %get-tuple-element.16, f32[32,256]{1,0:T(8,128)S(1)} %convolution_multiply_fusion.3, f32[32,256]{1,0:T(8,128)S(1)} %fusion.79, f32[32,128]{1,0:T(8,128)S(1)} %get-tuple-element.12, ...), kind=kLoop, calls=%fused_computation.10 | loop fusion | flops 6291456 | bytes 16941056 | tf_op jit(solution)/shard_map/add | solution.py:82
  303.1 2.6 collective-permute-done.8
  305.8 1.9 collective-permute-start.9
  307.8 0.7 pad_maximum_fusion.3
  308.5 3.9 %pad_maximum_fusion = f32[2,32,256,128]{3,2,1,0:T(8,128)} fusion(f32[1,32,256,128]{3,2,1,0:T(8,128)S(1)} %get-tuple-element.7, f32[1,32,256,128]{3,2,1,0:T(8,128)S(1)} %get-tuple-element.6), kind=kLoop, calls=%fused_computation | loop fusion | flops 2097152 | bytes 16777216 | tf_op jit(solution)/shard_map/stack | solution.py:100
  312.4 17.5 %collective-permute-done.9 = f32[32,4096]{1,0:T(8,128)S(1)} collective-permute-done((f32[32,4096]{1,0:T(8,128)S(1)}, f32[32,4096]{1,0:T(8,128)S(1)}, u32[]{:S(2)}, u32[]{:S(2)}) %collective-permute-start.9) | collective-permute-done | bytes 524320 | tf_op jit(solution)/shard_map/ppermute | solution.py:97
  330.0 0.8 fusion.61
  (60 shorter events, 1.7 us)
Async XLA Ops:
  0.6 10.9 %copy-start = (bf16[32,4096]{1,0:T(8,128)(2,1)S(1)}, bf16[32,4096]{1,0:T(8,128)(2,1)}, u32[]{:S(2)}) copy-start(bf16[32,4096]{1,0:T(8,128)(2,1)} %param.17) | copy-start | bytes 786436
  0.6 10.7 %copy-start.1 = (f32[2,32,2,256]{3,2,1,0:T(2,128)S(1)}, f32[2,32,2,256]{3,2,1,0:T(2,128)}, u32[]{:S(2)}) copy-start(f32[2,32,2,256]{3,2,1,0:T(2,128)} %param.32) | copy-start | bytes 393220
  0.7 10.7 %copy-start.10 = (f32[2,128]{1,0:T(2,128)S(1)}, f32[2,128]{1,0:T(2,128)}, u32[]{:S(2)}) copy-start(f32[2,128]{1,0:T(2,128)} %param.26) | copy-start | bytes 3076
  0.7 10.9 %copy-start.6 = (bf16[2,4096,128]{2,1,0:T(8,128)(2,1)S(1)}, bf16[2,4096,128]{2,1,0:T(8,128)(2,1)}, u32[]{:S(2)}) copy-start(bf16[2,4096,128]{2,1,0:T(8,128)(2,1)} %param.23) | copy-start | bytes 6291460
  0.7 11.9 %copy-start.2 = (f32[2,32,2,2,32]{4,3,2,1,0:T(2,128)S(1)}, f32[2,32,2,2,32]{4,3,2,1,0:T(2,128)}, u32[]{:S(2)}) copy-start(f32[2,32,2,2,32]{4,3,2,1,0:T(2,128)} %param.33) | copy-start | bytes 98308
  59.2 5.6 %copy-start.4 = (bf16[2,4096,256]{2,1,0:T(8,128)(2,1)S(1)}, bf16[2,4096,256]{2,1,0:T(8,128)(2,1)}, u32[]{:S(2)}) copy-start(bf16[2,4096,256]{2,1,0:T(8,128)(2,1)} %param.19) | copy-start | bytes 12582916
  104.7 68.4 %copy-start.8 = (bf16[2,4096,32]{1,2,0:T(8,128)(2,1)S(1)}, bf16[2,4096,32]{1,2,0:T(8,128)(2,1)}, u32[]{:S(2)}) copy-start(bf16[2,4096,32]{1,2,0:T(8,128)(2,1)} %param.22) | copy-start | bytes 1572868
  104.7 68.6 %copy-start.9 = (bf16[2,4096,32]{1,2,0:T(8,128)(2,1)S(1)}, bf16[2,4096,32]{1,2,0:T(8,128)(2,1)}, u32[]{:S(2)}) copy-start(bf16[2,4096,32]{1,2,0:T(8,128)(2,1)} %param.21) | copy-start | bytes 1572868
  104.7 2.0 collective-permute-start
  106.8 66.8 %copy-start.3 = (bf16[2,4096,256]{2,1,0:T(8,128)(2,1)S(1)}, bf16[2,4096,256]{2,1,0:T(8,128)(2,1)}, u32[]{:S(2)}) copy-start(bf16[2,4096,256]{2,1,0:T(8,128)(2,1)} %param.20) | copy-start | bytes 12582916
  106.8 14.6 %collective-permute-start.1 = (f32[32,4096]{1,0:T(8,128)S(1)}, f32[32,4096]{1,0:T(8,128)S(1)}, u32[]{:S(2)}, u32[]{:S(2)}) collective-permute-start(f32[32,4096]{1,0:T(8,128)S(1)} %add.167), channel_id=1, source_target_pairs={{0,2},{1,3},{2,0},{3,1},{4,6},{5,7},{6,4},{7,5},{8,10},{9,11},{10,... | collective-permute-start | bytes 1572872 | tf_op jit(solution)/shard_map/ppermute | solution.py:97
  121.4 52.6 %copy-start.7 = (bf16[2,4096,128]{2,1,0:T(8,128)(2,1)S(1)}, bf16[2,4096,128]{2,1,0:T(8,128)(2,1)}, u32[]{:S(2)}) copy-start(bf16[2,4096,128]{2,1,0:T(8,128)(2,1)} %param.23) | copy-start | bytes 6291460
  121.4 13.5 %collective-permute-start.2 = (f32[32,4096]{1,0:T(8,128)S(1)}, f32[32,4096]{1,0:T(8,128)S(1)}, u32[]{:S(2)}, u32[]{:S(2)}) collective-permute-start(f32[32,4096]{1,0:T(8,128)S(1)} %add.168), channel_id=1, source_target_pairs={{0,4},{1,5},{2,6},{3,7},{4,0},{5,1},{6,2},{7,3},{8,12},{9,13},{10,... | collective-permute-start | bytes 1572872 | tf_op jit(solution)/shard_map/ppermute | solution.py:97
  134.9 13.7 %collective-permute-start.3 = (f32[32,4096]{1,0:T(8,128)S(1)}, f32[32,4096]{1,0:T(8,128)S(1)}, u32[]{:S(2)}, u32[]{:S(2)}) collective-permute-start(f32[32,4096]{1,0:T(8,128)S(1)} %add.169), channel_id=1, source_target_pairs={{0,8},{1,9},{2,10},{3,11},{4,12},{5,13},{6,14},{7,15},{8,0},{9,1},... | collective-permute-start | bytes 1572872 | tf_op jit(solution)/shard_map/ppermute | solution.py:97
  148.7 24.2 %collective-permute-start.4 = (f32[32,4096]{1,0:T(8,128)S(1)}, f32[32,4096]{1,0:T(8,128)S(1)}, u32[]{:S(2)}, u32[]{:S(2)}) collective-permute-start(f32[32,4096]{1,0:T(8,128)S(1)} %add.170), channel_id=1, source_target_pairs={{0,16},{1,17},{2,18},{3,19},{4,20},{5,21},{6,22},{7,23},{8,24},{9,... | collective-permute-start | bytes 1572872 | tf_op jit(solution)/shard_map/ppermute | solution.py:97
  216.4 5.6 %copy-start.5 = (bf16[2,4096,256]{2,1,0:T(8,128)(2,1)S(1)}, bf16[2,4096,256]{2,1,0:T(8,128)(2,1)}, u32[]{:S(2)}) copy-start(bf16[2,4096,256]{2,1,0:T(8,128)(2,1)} %param.19) | copy-start | bytes 12582916
  261.9 1.9 collective-permute-start.5
  263.9 14.6 %collective-permute-start.6 = (f32[32,4096]{1,0:T(8,128)S(1)}, f32[32,4096]{1,0:T(8,128)S(1)}, u32[]{:S(2)}, u32[]{:S(2)}) collective-permute-start(f32[32,4096]{1,0:T(8,128)S(1)} %add.184), channel_id=1, source_target_pairs={{0,2},{1,3},{2,0},{3,1},{4,6},{5,7},{6,4},{7,5},{8,10},{9,11},{10,... | collective-permute-start | bytes 1572872 | tf_op jit(solution)/shard_map/ppermute | solution.py:97
  278.5 13.5 %collective-permute-start.7 = (f32[32,4096]{1,0:T(8,128)S(1)}, f32[32,4096]{1,0:T(8,128)S(1)}, u32[]{:S(2)}, u32[]{:S(2)}) collective-permute-start(f32[32,4096]{1,0:T(8,128)S(1)} %add.185), channel_id=1, source_target_pairs={{0,4},{1,5},{2,6},{3,7},{4,0},{5,1},{6,2},{7,3},{8,12},{9,13},{10,... | collective-permute-start | bytes 1572872 | tf_op jit(solution)/shard_map/ppermute | solution.py:97
  292.0 13.7 %collective-permute-start.8 = (f32[32,4096]{1,0:T(8,128)S(1)}, f32[32,4096]{1,0:T(8,128)S(1)}, u32[]{:S(2)}, u32[]{:S(2)}) collective-permute-start(f32[32,4096]{1,0:T(8,128)S(1)} %add.186), channel_id=1, source_target_pairs={{0,8},{1,9},{2,10},{3,11},{4,12},{5,13},{6,14},{7,15},{8,0},{9,1},... | collective-permute-start | bytes 1572872 | tf_op jit(solution)/shard_map/ppermute | solution.py:97
  305.8 24.2 %collective-permute-start.9 = (f32[32,4096]{1,0:T(8,128)S(1)}, f32[32,4096]{1,0:T(8,128)S(1)}, u32[]{:S(2)}, u32[]{:S(2)}) collective-permute-start(f32[32,4096]{1,0:T(8,128)S(1)} %add.187), channel_id=1, source_target_pairs={{0,16},{1,17},{2,18},{3,19},{4,20},{5,21},{6,22},{7,23},{8,24},{9,... | collective-permute-start | bytes 1572872 | tf_op jit(solution)/shard_map/ppermute | solution.py:97
